TPU v7x, 32 devices: a whole 2x2x4 slice. The times are simulated.
32 devices in a mesh: grp: 2 (over x), tp: 16 (over z, y, core).
Axes of the slice: x: 2, y: 2, z: 4, core: 2. Of those that a mesh axis runs over, the one named last changes fastest.
Arguments:
- tokens: bfloat16 [160, 2048], P('grp', 'tp'), parts along dimension 0, may hold values from -6 to 6
- lengths: int32 [160], P('grp'), parts along dimension 0, may hold values from 1 to 4096, 81920 in all
- cell_memory: float32 [2, 160, 2048, 256], P(None, 'grp', 'tp'), parts along dimension 1, may hold values from -0.6 to 0.6
- key_sums: float32 [2, 160, 2048], P(None, 'grp', 'tp'), parts along dimension 1, may hold values from -3 to 3
- stabilizer: float32 [2, 160, 8], P(None, 'grp'), parts along dimension 1, may hold values from -3 to 1
- norm_gain: bfloat16 [2, 2048], replicated, may hold values from 0.099609375 to 1.8984375
- query_weight: bfloat16 [2, 2048, 2048], P(None, None, 'tp'), may hold values from -0.125 to 0.125
- key_weight: bfloat16 [2, 2048, 2048], P(None, None, 'tp'), may hold values from -0.125 to 0.125
- value_weight: bfloat16 [2, 2048, 2048], P(None, None, 'tp'), may hold values from -0.125 to 0.125
- outgate_weight: bfloat16 [2, 2048, 2048], P(None, None, 'tp'), may hold values from -0.125 to 0.125
- ingate_weight: bfloat16 [2, 2048, 8], replicated, may hold values from -0.125 to 0.125
- forget_weight: bfloat16 [2, 2048, 8], replicated, may hold values from -0.125 to 0.125
- ingate_bias: float32 [2, 8], replicated, may hold values from -3 to 3
- forget_bias: float32 [2, 8], replicated, may hold values from -1 to 4
- forget_slope: float32 [2, 8], replicated, may hold values from -3 to 3
- head_gain: bfloat16 [2, 2048], P(None, 'tp'), may hold values from 0.099609375 to 1.8984375
- output_weight: bfloat16 [2, 2048, 2048], P(None, None, 'tp'), may hold values from -0.125 to 0.125
Outputs:
- new_tokens: bfloat16 [160, 2048], P('grp', 'tp'), parts along dimension 0
- new_memory: float32 [2, 160, 2048, 256], P(None, 'grp', 'tp'), parts along dimension 1
- new_key_sums: float32 [2, 160, 2048], P(None, 'grp', 'tp'), parts along dimension 1
- new_stabilizer: float32 [2, 160, 8], P(None, 'grp'), parts along dimension 1
There are 2 independent parts, one for each index of `grp`. A program takes and returns all parts, laid end to end along the dimension named above; an argument that names none is the same for every part. Nothing has to cross between parts.
Inputs may be any that keep to these rules, and one draw needn't show every extreme that they name: Each part's 80 lengths sum to 81920, and the largest is exactly 4096.
All inputs are finite; a program needn't handle non-finite values.
Results may differ from a plain program's by a relative error of at most 0.018.
Values may be sent and summed in bfloat16 or wider, within the bound.
A program may use at most 128 MiB of HBM per device.

v0:
```python
import jax
import jax.numpy as jnp
from jax import lax
from jax.sharding import PartitionSpec as P

HEADS = 8
HEAD = 256
MAXLEN = 4096
EPS = 1e-05


def from_partner(value, axis, stride):
    mask = 2**stride
    pairs = [(source, source ^ mask) for source in range(lax.axis_size(axis))]
    return lax.ppermute(value, axis, pairs)


def body(
    tokens,
    lengths,
    cell_memory,
    key_sums,
    stabilizer,
    norm_gain,
    query_weight,
    key_weight,
    value_weight,
    outgate_weight,
    ingate_weight,
    forget_weight,
    ingate_bias,
    forget_bias,
    forget_slope,
    head_gain,
    output_weight,
):
    devices = lax.axis_size("tp")
    split_count = devices // HEADS
    own_index = lax.axis_index("tp")
    head_id = own_index // split_count
    onehot = (jnp.arange(HEADS) == head_id).astype(jnp.float32)
    position = lengths.astype(jnp.float32) / MAXLEN
    current = tokens
    memories, sums_list, stabs = ([], [], [])
    for block_id in range(cell_memory.shape[0]):
        gathered_rows = lax.all_gather(current, "tp", axis=1, tiled=True)
        row_float = gathered_rows.astype(jnp.float32)
        normed = (
            row_float
            * lax.rsqrt(jnp.mean(row_float * row_float, axis=-1, keepdims=True) + EPS)
            * norm_gain[block_id].astype(jnp.float32)
        ).astype(jnp.bfloat16)
        queries = jnp.dot(
            normed, query_weight[block_id], preferred_element_type=jnp.float32
        ).astype(jnp.bfloat16)
        key_rows = (
            jnp.dot(normed, key_weight[block_id], preferred_element_type=jnp.float32)
            * HEAD ** (-0.5)
        ).astype(jnp.bfloat16)
        values = jnp.dot(normed, value_weight[block_id], preferred_element_type=jnp.float32).astype(
            jnp.bfloat16
        )
        outgate = jnp.dot(
            normed, outgate_weight[block_id], preferred_element_type=jnp.float32
        ).astype(jnp.bfloat16)
        ingate = (
            jnp.dot(normed, ingate_weight[block_id], preferred_element_type=jnp.float32)
            + ingate_bias[block_id]
        )
        forget = jax.nn.log_sigmoid(
            jnp.dot(normed, forget_weight[block_id], preferred_element_type=jnp.float32)
            + forget_bias[block_id]
            + forget_slope[block_id] * position[:, None]
        )
        stab_new = jnp.maximum(forget + stabilizer[block_id], ingate)
        decays = jnp.exp(forget + stabilizer[block_id] - stab_new)
        in_weight = jnp.exp(ingate - stab_new)
        decay_own = jnp.sum(decays * onehot, axis=1)
        inweight_own = jnp.sum(in_weight * onehot, axis=1)
        sums_new = decay_own[:, None] * key_sums[block_id] + inweight_own[
            :, None
        ] * key_rows.astype(jnp.float32)
        head_pair = jnp.stack((queries, key_rows))
        head_sums = sums_new
        for level in range(split_count.bit_length() - 1):
            partner = from_partner(head_pair, "tp", level)
            upper = own_index // (1 << level) % 2 == 1
            lower_half = jnp.where(upper, partner, head_pair)
            upper_half = jnp.where(upper, head_pair, partner)
            head_pair = jnp.concatenate((lower_half, upper_half), axis=2)
            sums_mate = from_partner(head_sums, "tp", level)
            sums_low = jnp.where(upper, sums_mate, head_sums)
            sums_high = jnp.where(upper, head_sums, sums_mate)
            head_sums = jnp.concatenate((sums_low, sums_high), axis=1)
        head_query = head_pair[0].astype(jnp.float32)
        head_keys = head_pair[1].astype(jnp.float32)
        mem_new = (
            decay_own[:, None, None] * cell_memory[block_id]
            + inweight_own[:, None, None]
            * values.astype(jnp.float32)[:, :, None]
            * head_keys[:, None, :]
        )
        numerator = jnp.einsum("bvk,bk->bv", mem_new, head_query, precision=lax.Precision.HIGHEST)
        denominator = jnp.maximum(jnp.abs(jnp.sum(head_sums * head_query, axis=1)), 1.0)
        hidden = numerator / denominator[:, None]
        gated_out = (
            hidden
            * head_gain[block_id].astype(jnp.float32)
            * jax.nn.sigmoid(outgate.astype(jnp.float32))
        ).astype(jnp.bfloat16)
        out_weight = output_weight[block_id]
        projected = jnp.dot(
            lax.all_gather(gated_out, "tp", axis=1, tiled=True),
            out_weight,
            preferred_element_type=jnp.float32,
        )
        current = (current.astype(jnp.float32) + projected).astype(jnp.bfloat16)
        memories.append(mem_new)
        sums_list.append(sums_new)
        stabs.append(stab_new)
    return (current, jnp.stack(memories), jnp.stack(sums_list), jnp.stack(stabs))


def solution(mesh):
    in_specs = (
        P("grp", "tp"),
        P("grp"),
        P(None, "grp", "tp", None),
        P(None, "grp", "tp"),
        P(None, "grp", None),
        P(),
        P(None, None, "tp"),
        P(None, None, "tp"),
        P(None, None, "tp"),
        P(None, None, "tp"),
        P(),
        P(),
        P(),
        P(),
        P(),
        P(None, "tp"),
        P(None, None, "tp"),
    )
    out_specs = (
        P("grp", "tp"),
        P(None, "grp", "tp", None),
        P(None, "grp", "tp"),
        P(None, "grp", None),
    )
    return jax.shard_map(body, mesh=mesh, in_specs=in_specs, out_specs=out_specs, check_vma=False)
```

profile of v0, /device:TPU:0, one launch (start us, length us, event | category | flops | bytes accessed | tf_op | source)
XLA Modules:
  0.0 133.5 jit_solution(18110746305476406706)
XLA Ops:
  0.7 0.7 convert_multiply_fusion.4
  1.3 0.8 slice_bitcast_fusion
  2.1 0.8 slice_convert_fusion
  2.9 24.3 %all_gather.12 = bf16[80,2048]{1,0:T(8,128)(2,1)S(1)} all-gather(bf16[80,128]{1,0:T(8,128)(2,1)} %param.17), channel_id=1, replica_groups=mesh['grp'=2,'tp'=16] {'tp'}, dimensions={1}, use_global_device_ids=true | all-gather | bytes 348160 | tf_op jit(solution)/shard_map/all_gather | solution.py:46
  27.3 0.8 slice_bitcast_fusion.1
  28.1 1.3 %fusion.38 = bf16[1,80,128]{2,1,0:T(8,128)(2,1)S(1)} fusion(bf16[2,2048,128]{2,1,0:T(8,128)(2,1)} %param.23, bf16[80,2048]{1,0:T(8,128)(2,1)S(1)} %all_gather.12, f32[2048]{0:T(1024)S(1)} %bitcast.144, f32[80]{0:T(128)S(1)} %add_rsqrt_fusion.1), kind=kOutput, calls=%fused_computation.51 | convolution fusion | flops 42608640 | bytes 880960 | tf_op jit(solution)/shard_map/dot_general | solution.py:53
  29.4 1.1 fusion.93
  30.6 1.1 multiply_reduce_fusion.3
  31.7 1.4 %fusion.81 = (f32[80,128]{1,0:T(8,128)S(1)}, bf16[80,128]{1,0:T(8,128)(2,1)S(1)}) fusion(f32[2,80,128]{2,1,0:T(8,128)} %param.20, f32[80]{0:T(128)S(1)} %get-tuple-element.6, f32[80]{0:T(128)S(1)} %get-tuple-element.7, bf16[2,2048,128]{2,1,0:T(8,128)(2,1)} %param.24, bf16[80,2048]{1,0:T(8,128)(2,1)S(1)} %all_gather.12, f32[2048]{0:T(1024)S(1)} %bitcast.147, ...), kind=kOutput, calls=%fused_computation.115 | convolution fusion | flops 42659840 | bytes 963520 | tf_op jit(solution)/shard_map/dot_general | solution.py:57
  33.1 0.4 collective-permute-start
  33.7 1.3 %fusion.37 = f32[80,128]{1,0:T(8,128)S(1)} fusion(bf16[2,2048,128]{2,1,0:T(8,128)(2,1)} %param.25, f32[80]{0:T(128)S(1)} %get-tuple-element.7, bf16[80,2048]{1,0:T(8,128)(2,1)S(1)} %all_gather.12, f32[2048]{0:T(1024)S(1)} %bitcast.148, f32[80]{0:T(128)S(1)} %add_rsqrt_fusion.1), kind=kOutput, calls=%fused_computation.50 | convolution fusion | flops 42629120 | bytes 901760 | tf_op jit(solution)/shard_map/dot_general | solution.py:60
  35.0 0.7 bitcast_convert_fusion
  36.0 8.7 %fusion.4 = f32[80,1,128]{2,1,0:T(1,128)S(1)} fusion(f32[2,80,128,256]{3,2,1,0:T(8,128)} %param.19, f32[80,256]{1,0:T(8,128)S(1)} %get-tuple-element.19, f32[80,128]{1,0:T(8,128)S(1)} %fusion.37, f32[80]{0:T(128)S(1)} %get-tuple-element.6, bf16[80,256,1]{1,0,2:T(8,128)(2,1)S(1)} %get-tuple-element.18), kind=kOutput, calls=%fused_computation.6 | convolution fusion | flops 39321600 | bytes 10690880 | tf_op jit(solution)/shard_map/bvk,bk->bv/dot_general | solution.py:103
  45.0 18.3 %all_gather.13 = bf16[80,2048]{1,0:T(8,128)(2,1)S(1)} all-gather(bf16[80,128]{1,0:T(8,128)(2,1)S(1)} %fusion.35), channel_id=1, replica_groups=mesh['grp'=2,'tp'=16] {'tp'}, dimensions={1}, use_global_device_ids=true | all-gather | bytes 348160 | tf_op jit(solution)/shard_map/all_gather | solution.py:113
  63.6 19.7 %all_gather.14 = bf16[80,2048]{1,0:T(8,128)(2,1)S(1)} all-gather(bf16[80,128]{1,0:T(8,128)(2,1)S(1)} %fusion.17), channel_id=1, replica_groups=mesh['grp'=2,'tp'=16] {'tp'}, dimensions={1}, use_global_device_ids=true | all-gather | bytes 348160 | tf_op jit(solution)/shard_map/all_gather | solution.py:46
  85.0 0.4 collective-permute-start.2
  85.6 0.6 pad_maximum_fusion.1
  86.3 0.6 pad_maximum_fusion.6
  87.1 10.3 %multiply_add_fusion.1 = (f32[1,80,128,256]{3,2,1,0:T(8,128)S(1)}, f32[1,80,128,256]{3,2,1,0:T(8,128)S(1)}) fusion(f32[2,80,128,256]{3,2,1,0:T(8,128)} %param.19, f32[80,256]{1,0:T(8,128)S(1)} %get-tuple-element.19, f32[80,128]{1,0:T(8,128)S(1)} %fusion.37, f32[80]{0:T(128)S(1)} %get-tuple-element.6, f32[80,256]{1,0:T(8,128)S(1)} %get-tuple-element.13, ...), kind=kLoop, calls=%fused_computation.8 | loop fusion | flops 15728640 | bytes 42189440 | tf_op jit(solution)/shard_map/add | solution.py:98
  97.4 8.6 %fusion.1 = f32[80,1,128]{2,1,0:T(1,128)S(1)} fusion(f32[2,80,128,256]{3,2,1,0:T(8,128)} %param.19, f32[80,256]{1,0:T(8,128)S(1)} %get-tuple-element.13, f32[80,128]{1,0:T(8,128)S(1)} %fusion.28, f32[80]{0:T(128)S(1)} %get-tuple-element.4, bf16[80,256,1]{1,0,2:T(8,128)(2,1)S(1)} %get-tuple-element.12), kind=kOutput, calls=%fused_computation.3 | convolution fusion | flops 39321600 | bytes 10690880 | tf_op jit(solution)/shard_map/bvk,bk->bv/dot_general | solution.py:103
  106.0 0.3 fusion.26
  106.3 18.3 %all_gather.15 = bf16[80,2048]{1,0:T(8,128)(2,1)S(1)} all-gather(bf16[80,128]{1,0:T(8,128)(2,1)S(1)} %fusion.26), channel_id=1, replica_groups=mesh['grp'=2,'tp'=16] {'tp'}, dimensions={1}, use_global_device_ids=true | all-gather | bytes 348160 | tf_op jit(solution)/shard_map/all_gather | solution.py:113
  124.6 0.9 fusion.19
  125.5 8.0 %pad_maximum_fusion = f32[2,80,128,256]{3,2,1,0:T(8,128)} fusion(f32[1,80,128,256]{3,2,1,0:T(8,128)S(1)} %get-tuple-element.9, f32[1,80,128,256]{3,2,1,0:T(8,128)S(1)} %get-tuple-element.8), kind=kLoop, calls=%fused_computation | loop fusion | flops 5242880 | bytes 41943040 | tf_op jit(solution)/shard_map/stack | solution.py:121
  (50 shorter events, 3.1 us)
Async XLA Ops:
  27.1 36.2 %copy-start = (bf16[80,128]{1,0:T(8,128)(2,1)S(1)}, bf16[80,128]{1,0:T(8,128)(2,1)}, u32[]{:S(2)}) copy-start(bf16[80,128]{1,0:T(8,128)(2,1)} %param.17) | copy-start | bytes 61444
  29.4 54.0 %copy-start.1 = (bf16[2,2048,128]{2,1,0:T(8,128)(2,1)S(1)}, bf16[2,2048,128]{2,1,0:T(8,128)(2,1)}, u32[]{:S(2)}) copy-start(bf16[2,2048,128]{2,1,0:T(8,128)(2,1)} %param.23) | copy-start | bytes 3145732
  31.6 52.1 %copy-start.7 = (bf16[2,2048,8]{1,2,0:T(8,128)(2,1)S(1)}, bf16[2,2048,8]{1,2,0:T(8,128)(2,1)}, u32[]{:S(2)}) copy-start(bf16[2,2048,8]{1,2,0:T(8,128)(2,1)} %param.28) | copy-start | bytes 196612
  31.6 52.1 %copy-start.9 = (f32[2,80,8]{1,2,0:T(8,128)S(1)}, f32[2,80,8]{1,2,0:T(8,128)}, u32[]{:S(2)}) copy-start(f32[2,80,8]{1,2,0:T(8,128)} %param.21) | copy-start | bytes 15364
  31.7 52.4 %copy-start.8 = (bf16[2,2048,8]{1,2,0:T(8,128)(2,1)S(1)}, bf16[2,2048,8]{1,2,0:T(8,128)(2,1)}, u32[]{:S(2)}) copy-start(bf16[2,2048,8]{1,2,0:T(8,128)(2,1)} %param.27) | copy-start | bytes 196612
  33.1 51.3 %copy-start.2 = (bf16[2,2048,128]{2,1,0:T(8,128)(2,1)S(1)}, bf16[2,2048,128]{2,1,0:T(8,128)(2,1)}, u32[]{:S(2)}) copy-start(bf16[2,2048,128]{2,1,0:T(8,128)(2,1)} %param.25) | copy-start | bytes 3145732
  33.1 2.7 %collective-permute-start = (bf16[2,80,128]{2,1,0:T(8,128)(2,1)S(1)}, bf16[2,80,128]{2,1,0:T(8,128)(2,1)S(1)}, u32[]{:S(2)}, u32[]{:S(2)}) collective-permute-start(bf16[2,80,128]{2,1,0:T(8,128)(2,1)S(1)} %pad_maximum_fusion.4), channel_id=1, source_target_pairs={{0,1},{1,0},{2,3},{3,2},{4,5},{5,4},{6,7},{7,6},{8,9},{9,8},{10,11... | collective-permute-start | bytes 122888 | tf_op jit(solution)/shard_map/ppermute | solution.py:15
  33.5 2.3 %collective-permute-start.1 = (f32[80,128]{1,0:T(8,128)S(1)}, f32[80,128]{1,0:T(8,128)S(1)}, u32[]{:S(2)}, u32[]{:S(2)}) collective-permute-start(f32[80,128]{1,0:T(8,128)S(1)} %get-tuple-element.34), channel_id=1, source_target_pairs={{0,1},{1,0},{2,3},{3,2},{4,5},{5,4},{6,7},{7,6},{8,9},{9,8},{10,11... | collective-permute-start | bytes 122888 | tf_op jit(solution)/shard_map/ppermute | solution.py:15
  35.0 49.7 %copy-start.6 = (f32[2,80,128]{2,1,0:T(8,128)S(1)}, f32[2,80,128]{2,1,0:T(8,128)}, u32[]{:S(2)}) copy-start(f32[2,80,128]{2,1,0:T(8,128)} %param.20) | copy-start | bytes 245764
  35.8 8.9 %copy-start.4 = (bf16[2,2048,128]{2,1,0:T(8,128)(2,1)S(1)}, bf16[2,2048,128]{2,1,0:T(8,128)(2,1)}, u32[]{:S(2)}) copy-start(bf16[2,2048,128]{2,1,0:T(8,128)(2,1)} %param.26) | copy-start | bytes 3145732
  35.8 27.6 %copy-start.5 = (bf16[2,2048,128]{2,1,0:T(8,128)(2,1)S(1)}, bf16[2,2048,128]{2,1,0:T(8,128)(2,1)}, u32[]{:S(2)}) copy-start(bf16[2,2048,128]{2,1,0:T(8,128)(2,1)} %param.33) | copy-start | bytes 3145732
  35.8 48.9 %copy-start.3 = (bf16[2,2048,128]{2,1,0:T(8,128)(2,1)S(1)}, bf16[2,2048,128]{2,1,0:T(8,128)(2,1)}, u32[]{:S(2)}) copy-start(bf16[2,2048,128]{2,1,0:T(8,128)(2,1)} %param.24) | copy-start | bytes 3145732
  85.0 1.8 %collective-permute-start.2 = (bf16[2,80,128]{2,1,0:T(8,128)(2,1)S(1)}, bf16[2,80,128]{2,1,0:T(8,128)(2,1)S(1)}, u32[]{:S(2)}, u32[]{:S(2)}) collective-permute-start(bf16[2,80,128]{2,1,0:T(8,128)(2,1)S(1)} %pad_maximum_fusion.5), channel_id=1, source_target_pairs={{0,1},{1,0},{2,3},{3,2},{4,5},{5,4},{6,7},{7,6},{8,9},{9,8},{10,11... | collective-permute-start | bytes 122888 | tf_op jit(solution)/shard_map/ppermute | solution.py:15
  85.5 1.4 %collective-permute-start.3 = (f32[80,128]{1,0:T(8,128)S(1)}, f32[80,128]{1,0:T(8,128)S(1)}, u32[]{:S(2)}, u32[]{:S(2)}) collective-permute-start(f32[80,128]{1,0:T(8,128)S(1)} %get-tuple-element.36), channel_id=1, source_target_pairs={{0,1},{1,0},{2,3},{3,2},{4,5},{5,4},{6,7},{7,6},{8,9},{9,8},{10,11... | collective-permute-start | bytes 122888 | tf_op jit(solution)/shard_map/ppermute | solution.py:15
where the time goes:
time: 134 us; the launch traced here: 133 us
  blocking collectives  80.6 us (60%)
  matrix products  26.8 us (20%)
  other arithmetic  22.4 us (17%)
  local copies, waits for them, and re-layouts  1.58 us (1%)
    all_gather x2, blocking collectives, body(): gathered_rows = lax.all_gather(current, 'tp', axis=1, tiled=True)  43.9 us
    all_gather x2, blocking collectives, body(): lax.all_gather(gated_out, 'tp', axis=1, tiled=True)  36.7 us
    dot_general x2, matrix products, body(): jnp.einsum('bvk,bk->bv', mem_new, head_query, precision=lax.Precision.HIG...  17.2 us
    add x1, other arithmetic, body(): decay_own[:, None, None] * cell_memory[block_id]  10.3 us
    another operation x1, other arithmetic, body(): jnp.stack(memories)  8 us
  transfers between devices with their start and end apart: 4, of which 0 were waited for; matrix products, arithmetic and copies ran while one was open for 3% of the time, Pallas kernels for 0%

commit v1 on v0

--- a/solution.py
+++ b/solution.py
@@ -43,7 +43,14 @@
     current = tokens
     memories, sums_list, stabs = ([], [], [])
     for block_id in range(cell_memory.shape[0]):
-        gathered_rows = lax.all_gather(current, "tp", axis=1, tiled=True)
+        ring = [current]
+        for hop in range(15):
+            ring.append(lax.ppermute(ring[-1], "tp", [(dev, (dev + 1) % 16) for dev in range(16)]))
+        gathered_rows = jnp.roll(
+            jnp.concatenate(ring[::-1], axis=1),
+            (lax.axis_index("tp") + 1) * ring[0].shape[1],
+            axis=1,
+        )
         row_float = gathered_rows.astype(jnp.float32)
         normed = (
             row_float

time: 134 us -> 267 us (1.99)
  waiting for transfers between devices: 0.01 us -> 175 us
  blocking collectives: 80.6 us -> 36.4 us
    ppermute x0 -> x30, waiting for transfers between devices: none -> 174 us  [body(): lax.ppermute(ring[-1], 'tp', [(dev, (dev + 1) % 16) for dev in range(16)])]
    all_gather x2 -> x0, blocking collectives: 43.9 us -> none  [body(): gathered_rows = lax.all_gather(current, 'tp', axis=1, tiled=True)]
  transfers between devices with their start and end apart: 4 -> 34, of which waited for: 0 -> 31; matrix products, arithmetic and copies ran while one was open for 3% -> 2% of each run, Pallas kernels for 0% -> 0%
where the time goes in v1:
time: 267 us; the launch traced here: 266 us
  waiting for transfers between devices  175 us (66%)
  blocking collectives  36.4 us (14%)
  matrix products  26 us (10%)
  other arithmetic  23.2 us (9%)
  local copies, waits for them, and re-layouts  2.67 us (1%)
    ppermute x30, waiting for transfers between devices, body(): lax.ppermute(ring[-1], 'tp', [(dev, (dev + 1) % 16) for dev in range(16)])  174 us
    all_gather x2, blocking collectives, body(): lax.all_gather(gated_out, 'tp', axis=1, tiled=True)  36.4 us
    dot_general x2, matrix products, body(): jnp.einsum('bvk,bk->bv', mem_new, head_query, precision=lax.Precision.HIG...  17.1 us
    add x1, other arithmetic, body(): decay_own[:, None, None] * cell_memory[block_id]  10.3 us
    another operation x1, other arithmetic, body(): jnp.stack(memories)  8 us
  transfers between devices with their start and end apart: 34, of which 31 were waited for; matrix products, arithmetic and copies ran while one was open for 2% of the time, Pallas kernels for 0%

profile of v1, /device:TPU:0, one launch (start us, length us, event | category | flops | bytes accessed | tf_op | source)
XLA Modules:
  0.0 266.1 jit_solution(772104936711962558)
XLA Ops:
  1.2 6.7 %collective-permute-done = bf16[80,128]{1,0:T(8,128)(2,1)S(1)} collective-permute-done((bf16[80,128]{1,0:T(8,128)(2,1)}, bf16[80,128]{1,0:T(8,128)(2,1)S(1)}, u32[]{:S(2)}, u32[]{:S(2)}) %collective-permute-start) | collective-permute-done | bytes 20512 | tf_op jit(solution)/shard_map/ppermute | solution.py:48
  7.9 5.9 %collective-permute-done.1 = bf16[80,128]{1,0:T(8,128)(2,1)S(1)} collective-permute-done((bf16[80,128]{1,0:T(8,128)(2,1)S(1)}, bf16[80,128]{1,0:T(8,128)(2,1)S(1)}, u32[]{:S(2)}, u32[]{:S(2)}) %collective-permute-start.1) | collective-permute-done | bytes 20512 | tf_op jit(solution)/shard_map/ppermute | solution.py:48
  13.8 5.9 %collective-permute-done.2 = bf16[80,128]{1,0:T(8,128)(2,1)S(1)} collective-permute-done((bf16[80,128]{1,0:T(8,128)(2,1)S(1)}, bf16[80,128]{1,0:T(8,128)(2,1)S(1)}, u32[]{:S(2)}, u32[]{:S(2)}) %collective-permute-start.2) | collective-permute-done | bytes 20512 | tf_op jit(solution)/shard_map/ppermute | solution.py:48
  19.7 5.9 %collective-permute-done.3 = bf16[80,128]{1,0:T(8,128)(2,1)S(1)} collective-permute-done((bf16[80,128]{1,0:T(8,128)(2,1)S(1)}, bf16[80,128]{1,0:T(8,128)(2,1)S(1)}, u32[]{:S(2)}, u32[]{:S(2)}) %collective-permute-start.3) | collective-permute-done | bytes 20512 | tf_op jit(solution)/shard_map/ppermute | solution.py:48
  25.6 5.9 %collective-permute-done.4 = bf16[80,128]{1,0:T(8,128)(2,1)S(1)} collective-permute-done((bf16[80,128]{1,0:T(8,128)(2,1)S(1)}, bf16[80,128]{1,0:T(8,128)(2,1)S(1)}, u32[]{:S(2)}, u32[]{:S(2)}) %collective-permute-start.4) | collective-permute-done | bytes 20512 | tf_op jit(solution)/shard_map/ppermute | solution.py:48
  31.5 5.9 %collective-permute-done.5 = bf16[80,128]{1,0:T(8,128)(2,1)S(1)} collective-permute-done((bf16[80,128]{1,0:T(8,128)(2,1)S(1)}, bf16[80,128]{1,0:T(8,128)(2,1)S(1)}, u32[]{:S(2)}, u32[]{:S(2)}) %collective-permute-start.5) | collective-permute-done | bytes 20512 | tf_op jit(solution)/shard_map/ppermute | solution.py:48
  37.4 5.9 %collective-permute-done.6 = bf16[80,128]{1,0:T(8,128)(2,1)S(1)} collective-permute-done((bf16[80,128]{1,0:T(8,128)(2,1)S(1)}, bf16[80,128]{1,0:T(8,128)(2,1)S(1)}, u32[]{:S(2)}, u32[]{:S(2)}) %collective-permute-start.6) | collective-permute-done | bytes 20512 | tf_op jit(solution)/shard_map/ppermute | solution.py:48
  43.3 5.9 %collective-permute-done.7 = bf16[80,128]{1,0:T(8,128)(2,1)S(1)} collective-permute-done((bf16[80,128]{1,0:T(8,128)(2,1)S(1)}, bf16[80,128]{1,0:T(8,128)(2,1)S(1)}, u32[]{:S(2)}, u32[]{:S(2)}) %collective-permute-start.7) | collective-permute-done | bytes 20512 | tf_op jit(solution)/shard_map/ppermute | solution.py:48
  49.2 5.9 %collective-permute-done.8 = bf16[80,128]{1,0:T(8,128)(2,1)S(1)} collective-permute-done((bf16[80,128]{1,0:T(8,128)(2,1)S(1)}, bf16[80,128]{1,0:T(8,128)(2,1)S(1)}, u32[]{:S(2)}, u32[]{:S(2)}) %collective-permute-start.8) | collective-permute-done | bytes 20512 | tf_op jit(solution)/shard_map/ppermute | solution.py:48
  99.9 8.6 %fusion.4 = f32[80,1,128]{2,1,0:T(1,128)S(1)} fusion(f32[2,80,128,256]{3,2,1,0:T(8,128)} %param.21, f32[80,256]{1,0:T(8,128)S(1)} %get-tuple-element.20, f32[80,128]{1,0:T(8,128)S(1)} %fusion.37, f32[80]{0:T(128)S(1)} %get-tuple-element.7, bf16[80,256,1]{1,0,2:T(8,128)(2,1)S(1)} %get-tuple-element.19), kind=kOutput, calls=%fused_computation.6 | convolution fusion | flops 39321600 | bytes 10690880 | tf_op jit(solution)/shard_map/bvk,bk->bv/dot_general | solution.py:110
  108.7 18.3 %all_gather.6 = bf16[80,2048]{1,0:T(8,128)(2,1)S(1)} all-gather(bf16[80,128]{1,0:T(8,128)(2,1)S(1)} %fusion.35), channel_id=1, replica_groups=mesh['grp'=2,'tp'=16] {'tp'}, dimensions={1}, use_global_device_ids=true | all-gather | bytes 348160 | tf_op jit(solution)/shard_map/all_gather | solution.py:120
  133.3 5.9 %collective-permute-done.18 = bf16[80,128]{1,0:T(8,128)(2,1)S(1)} collective-permute-done((bf16[80,128]{1,0:T(8,128)(2,1)S(1)}, bf16[80,128]{1,0:T(8,128)(2,1)S(1)}, u32[]{:S(2)}, u32[]{:S(2)}) %collective-permute-start.18) | collective-permute-done | bytes 20512 | tf_op jit(solution)/shard_map/ppermute | solution.py:48
  139.2 5.9 %collective-permute-done.19 = bf16[80,128]{1,0:T(8,128)(2,1)S(1)} collective-permute-done((bf16[80,128]{1,0:T(8,128)(2,1)S(1)}, bf16[80,128]{1,0:T(8,128)(2,1)S(1)}, u32[]{:S(2)}, u32[]{:S(2)}) %collective-permute-start.19) | collective-permute-done | bytes 20512 | tf_op jit(solution)/shard_map/ppermute | solution.py:48
  145.1 5.9 %collective-permute-done.20 = bf16[80,128]{1,0:T(8,128)(2,1)S(1)} collective-permute-done((bf16[80,128]{1,0:T(8,128)(2,1)S(1)}, bf16[80,128]{1,0:T(8,128)(2,1)S(1)}, u32[]{:S(2)}, u32[]{:S(2)}) %collective-permute-start.20) | collective-permute-done | bytes 20512 | tf_op jit(solution)/shard_map/ppermute | solution.py:48
  151.0 5.9 %collective-permute-done.21 = bf16[80,128]{1,0:T(8,128)(2,1)S(1)} collective-permute-done((bf16[80,128]{1,0:T(8,128)(2,1)S(1)}, bf16[80,128]{1,0:T(8,128)(2,1)S(1)}, u32[]{:S(2)}, u32[]{:S(2)}) %collective-permute-start.21) | collective-permute-done | bytes 20512 | tf_op jit(solution)/shard_map/ppermute | solution.py:48
  156.9 5.9 %collective-permute-done.22 = bf16[80,128]{1,0:T(8,128)(2,1)S(1)} collective-permute-done((bf16[80,128]{1,0:T(8,128)(2,1)S(1)}, bf16[80,128]{1,0:T(8,128)(2,1)S(1)}, u32[]{:S(2)}, u32[]{:S(2)}) %collective-permute-start.22) | collective-permute-done | bytes 20512 | tf_op jit(solution)/shard_map/ppermute | solution.py:48
  162.8 5.9 %collective-permute-done.23 = bf16[80,128]{1,0:T(8,128)(2,1)S(1)} collective-permute-done((bf16[80,128]{1,0:T(8,128)(2,1)S(1)}, bf16[80,128]{1,0:T(8,128)(2,1)S(1)}, u32[]{:S(2)}, u32[]{:S(2)}) %collective-permute-start.23) | collective-permute-done | bytes 20512 | tf_op jit(solution)/shard_map/ppermute | solution.py:48
  168.7 5.9 %collective-permute-done.24 = bf16[80,128]{1,0:T(8,128)(2,1)S(1)} collective-permute-done((bf16[80,128]{1,0:T(8,128)(2,1)S(1)}, bf16[80,128]{1,0:T(8,128)(2,1)S(1)}, u32[]{:S(2)}, u32[]{:S(2)}) %collective-permute-start.24) | collective-permute-done | bytes 20512 | tf_op jit(solution)/shard_map/ppermute | solution.py:48
  174.6 5.9 %collective-permute-done.25 = bf16[80,128]{1,0:T(8,128)(2,1)S(1)} collective-permute-done((bf16[80,128]{1,0:T(8,128)(2,1)S(1)}, bf16[80,128]{1,0:T(8,128)(2,1)S(1)}, u32[]{:S(2)}, u32[]{:S(2)}) %collective-permute-start.25) | collective-permute-done | bytes 20512 | tf_op jit(solution)/shard_map/ppermute | solution.py:48
  180.5 5.9 %collective-permute-done.26 = bf16[80,128]{1,0:T(8,128)(2,1)S(1)} collective-permute-done((bf16[80,128]{1,0:T(8,128)(2,1)S(1)}, bf16[80,128]{1,0:T(8,128)(2,1)S(1)}, u32[]{:S(2)}, u32[]{:S(2)}) %collective-permute-start.26) | collective-permute-done | bytes 20512 | tf_op jit(solution)/shard_map/ppermute | solution.py:48
  220.0 10.3 %multiply_add_fusion.1 = (f32[1,80,128,256]{3,2,1,0:T(8,128)S(1)}, f32[1,80,128,256]{3,2,1,0:T(8,128)S(1)}) fusion(f32[2,80,128,256]{3,2,1,0:T(8,128)} %param.21, f32[80,256]{1,0:T(8,128)S(1)} %get-tuple-element.20, f32[80,128]{1,0:T(8,128)S(1)} %fusion.37, f32[80]{0:T(128)S(1)} %get-tuple-element.7, f32[80,256]{1,0:T(8,128)S(1)} %get-tuple-element.14, ...), kind=kLoop, calls=%fused_computation.8 | loop fusion | flops 15728640 | bytes 42189440 | tf_op jit(solution)/shard_map/add | solution.py:105
  230.4 8.5 %fusion.1 = f32[80,1,128]{2,1,0:T(1,128)S(1)} fusion(f32[2,80,128,256]{3,2,1,0:T(8,128)} %param.21, f32[80,256]{1,0:T(8,128)S(1)} %get-tuple-element.14, f32[80,128]{1,0:T(8,128)S(1)} %fusion.28, f32[80]{0:T(128)S(1)} %get-tuple-element.5, bf16[80,256,1]{1,0,2:T(8,128)(2,1)S(1)} %get-tuple-element.13), kind=kOutput, calls=%fused_computation.3 | convolution fusion | flops 39321600 | bytes 10690880 | tf_op jit(solution)/shard_map/bvk,bk->bv/dot_general | solution.py:110
  239.2 18.1 %all_gather.7 = bf16[80,2048]{1,0:T(8,128)(2,1)S(1)} all-gather(bf16[80,128]{1,0:T(8,128)(2,1)S(1)} %fusion.26), channel_id=1, replica_groups=mesh['grp'=2,'tp'=16] {'tp'}, dimensions={1}, use_global_device_ids=true | all-gather | bytes 348160 | tf_op jit(solution)/shard_map/all_gather | solution.py:120
  258.1 8.0 %pad_maximum_fusion = f32[2,80,128,256]{3,2,1,0:T(8,128)} fusion(f32[1,80,128,256]{3,2,1,0:T(8,128)S(1)} %get-tuple-element.10, f32[1,80,128,256]{3,2,1,0:T(8,128)S(1)} %get-tuple-element.9), kind=kLoop, calls=%fused_computation | loop fusion | flops 5242880 | bytes 41943040 | tf_op jit(solution)/shard_map/stack | solution.py:128
  (142 shorter events, 86.2 us)
Async XLA Ops:
  0.7 7.2 %collective-permute-start = (bf16[80,128]{1,0:T(8,128)(2,1)}, bf16[80,128]{1,0:T(8,128)(2,1)S(1)}, u32[]{:S(2)}, u32[]{:S(2)}) collective-permute-start(bf16[80,128]{1,0:T(8,128)(2,1)} %param.19), channel_id=1, source_target_pairs={{0,1},{1,2},{2,3},{3,4},{4,5},{5,6},{6,7},{7,8},{8,9},{9,10},{10,1... | collective-permute-start | bytes 61448 | tf_op jit(solution)/shard_map/ppermute | solution.py:48
  7.9 5.9 %collective-permute-start.1 = (bf16[80,128]{1,0:T(8,128)(2,1)S(1)}, bf16[80,128]{1,0:T(8,128)(2,1)S(1)}, u32[]{:S(2)}, u32[]{:S(2)}) collective-permute-start(bf16[80,128]{1,0:T(8,128)(2,1)S(1)} %collective-permute-done), channel_id=1, source_target_pairs={{0,1},{1,2},{2,3},{3,4},{4,5},{5,6},{6,7},{7,8},{8,9},{9,10},{10,1... | collective-permute-start | bytes 61448 | tf_op jit(solution)/shard_map/ppermute | solution.py:48
  13.8 5.9 %collective-permute-start.2 = (bf16[80,128]{1,0:T(8,128)(2,1)S(1)}, bf16[80,128]{1,0:T(8,128)(2,1)S(1)}, u32[]{:S(2)}, u32[]{:S(2)}) collective-permute-start(bf16[80,128]{1,0:T(8,128)(2,1)S(1)} %collective-permute-done.1), channel_id=1, source_target_pairs={{0,1},{1,2},{2,3},{3,4},{4,5},{5,6},{6,7},{7,8},{8,9},{9,10},{10,1... | collective-permute-start | bytes 61448 | tf_op jit(solution)/shard_map/ppermute | solution.py:48
  19.7 5.9 %collective-permute-start.3 = (bf16[80,128]{1,0:T(8,128)(2,1)S(1)}, bf16[80,128]{1,0:T(8,128)(2,1)S(1)}, u32[]{:S(2)}, u32[]{:S(2)}) collective-permute-start(bf16[80,128]{1,0:T(8,128)(2,1)S(1)} %collective-permute-done.2), channel_id=1, source_target_pairs={{0,1},{1,2},{2,3},{3,4},{4,5},{5,6},{6,7},{7,8},{8,9},{9,10},{10,1... | collective-permute-start | bytes 61448 | tf_op jit(solution)/shard_map/ppermute | solution.py:48
  25.6 5.9 %collective-permute-start.4 = (bf16[80,128]{1,0:T(8,128)(2,1)S(1)}, bf16[80,128]{1,0:T(8,128)(2,1)S(1)}, u32[]{:S(2)}, u32[]{:S(2)}) collective-permute-start(bf16[80,128]{1,0:T(8,128)(2,1)S(1)} %collective-permute-done.3), channel_id=1, source_target_pairs={{0,1},{1,2},{2,3},{3,4},{4,5},{5,6},{6,7},{7,8},{8,9},{9,10},{10,1... | collective-permute-start | bytes 61448 | tf_op jit(solution)/shard_map/ppermute | solution.py:48
  31.5 5.9 %collective-permute-start.5 = (bf16[80,128]{1,0:T(8,128)(2,1)S(1)}, bf16[80,128]{1,0:T(8,128)(2,1)S(1)}, u32[]{:S(2)}, u32[]{:S(2)}) collective-permute-start(bf16[80,128]{1,0:T(8,128)(2,1)S(1)} %collective-permute-done.4), channel_id=1, source_target_pairs={{0,1},{1,2},{2,3},{3,4},{4,5},{5,6},{6,7},{7,8},{8,9},{9,10},{10,1... | collective-permute-start | bytes 61448 | tf_op jit(solution)/shard_map/ppermute | solution.py:48
  43.3 5.9 %collective-permute-start.7 = (bf16[80,128]{1,0:T(8,128)(2,1)S(1)}, bf16[80,128]{1,0:T(8,128)(2,1)S(1)}, u32[]{:S(2)}, u32[]{:S(2)}) collective-permute-start(bf16[80,128]{1,0:T(8,128)(2,1)S(1)} %collective-permute-done.6), channel_id=1, source_target_pairs={{0,1},{1,2},{2,3},{3,4},{4,5},{5,6},{6,7},{7,8},{8,9},{9,10},{10,1... | collective-permute-start | bytes 61448 | tf_op jit(solution)/shard_map/ppermute | solution.py:48
  49.2 5.9 %collective-permute-start.8 = (bf16[80,128]{1,0:T(8,128)(2,1)S(1)}, bf16[80,128]{1,0:T(8,128)(2,1)S(1)}, u32[]{:S(2)}, u32[]{:S(2)}) collective-permute-start(bf16[80,128]{1,0:T(8,128)(2,1)S(1)} %collective-permute-done.7), channel_id=1, source_target_pairs={{0,1},{1,2},{2,3},{3,4},{4,5},{5,6},{6,7},{7,8},{8,9},{9,10},{10,1... | collective-permute-start | bytes 61448 | tf_op jit(solution)/shard_map/ppermute | solution.py:48
  55.1 5.9 %collective-permute-start.9 = (bf16[80,128]{1,0:T(8,128)(2,1)S(1)}, bf16[80,128]{1,0:T(8,128)(2,1)S(1)}, u32[]{:S(2)}, u32[]{:S(2)}) collective-permute-start(bf16[80,128]{1,0:T(8,128)(2,1)S(1)} %collective-permute-done.8), channel_id=1, source_target_pairs={{0,1},{1,2},{2,3},{3,4},{4,5},{5,6},{6,7},{7,8},{8,9},{9,10},{10,1... | collective-permute-start | bytes 61448 | tf_op jit(solution)/shard_map/ppermute | solution.py:48
  61.0 5.9 %collective-permute-start.10 = (bf16[80,128]{1,0:T(8,128)(2,1)S(1)}, bf16[80,128]{1,0:T(8,128)(2,1)S(1)}, u32[]{:S(2)}, u32[]{:S(2)}) collective-permute-start(bf16[80,128]{1,0:T(8,128)(2,1)S(1)} %collective-permute-done.9), channel_id=1, source_target_pairs={{0,1},{1,2},{2,3},{3,4},{4,5},{5,6},{6,7},{7,8},{8,9},{9,10},{10,1... | collective-permute-start | bytes 61448 | tf_op jit(solution)/shard_map/ppermute | solution.py:48
  66.9 5.9 %collective-permute-start.11 = (bf16[80,128]{1,0:T(8,128)(2,1)S(1)}, bf16[80,128]{1,0:T(8,128)(2,1)S(1)}, u32[]{:S(2)}, u32[]{:S(2)}) collective-permute-start(bf16[80,128]{1,0:T(8,128)(2,1)S(1)} %collective-permute-done.10), channel_id=1, source_target_pairs={{0,1},{1,2},{2,3},{3,4},{4,5},{5,6},{6,7},{7,8},{8,9},{9,10},{10,1... | collective-permute-start | bytes 61448 | tf_op jit(solution)/shard_map/ppermute | solution.py:48
  72.8 5.9 %collective-permute-start.12 = (bf16[80,128]{1,0:T(8,128)(2,1)S(1)}, bf16[80,128]{1,0:T(8,128)(2,1)S(1)}, u32[]{:S(2)}, u32[]{:S(2)}) collective-permute-start(bf16[80,128]{1,0:T(8,128)(2,1)S(1)} %collective-permute-done.11), channel_id=1, source_target_pairs={{0,1},{1,2},{2,3},{3,4},{4,5},{5,6},{6,7},{7,8},{8,9},{9,10},{10,1... | collective-permute-start | bytes 61448 | tf_op jit(solution)/shard_map/ppermute | solution.py:48
  84.6 5.9 %collective-permute-start.14 = (bf16[80,128]{1,0:T(8,128)(2,1)S(1)}, bf16[80,128]{1,0:T(8,128)(2,1)S(1)}, u32[]{:S(2)}, u32[]{:S(2)}) collective-permute-start(bf16[80,128]{1,0:T(8,128)(2,1)S(1)} %collective-permute-done.13), channel_id=1, source_target_pairs={{0,1},{1,2},{2,3},{3,4},{4,5},{5,6},{6,7},{7,8},{8,9},{9,10},{10,1... | collective-permute-start | bytes 61448 | tf_op jit(solution)/shard_map/ppermute | solution.py:48
  127.3 6.0 %collective-permute-start.17 = (bf16[80,128]{1,0:T(8,128)(2,1)S(1)}, bf16[80,128]{1,0:T(8,128)(2,1)S(1)}, u32[]{:S(2)}, u32[]{:S(2)}) collective-permute-start(bf16[80,128]{1,0:T(8,128)(2,1)S(1)} %fusion.17), channel_id=1, source_target_pairs={{0,1},{1,2},{2,3},{3,4},{4,5},{5,6},{6,7},{7,8},{8,9},{9,10},{10,1... | collective-permute-start | bytes 61448 | tf_op jit(solution)/shard_map/ppermute | solution.py:48
  133.3 5.9 %collective-permute-start.18 = (bf16[80,128]{1,0:T(8,128)(2,1)S(1)}, bf16[80,128]{1,0:T(8,128)(2,1)S(1)}, u32[]{:S(2)}, u32[]{:S(2)}) collective-permute-start(bf16[80,128]{1,0:T(8,128)(2,1)S(1)} %collective-permute-done.17), channel_id=1, source_target_pairs={{0,1},{1,2},{2,3},{3,4},{4,5},{5,6},{6,7},{7,8},{8,9},{9,10},{10,1... | collective-permute-start | bytes 61448 | tf_op jit(solution)/shard_map/ppermute | solution.py:48
  139.2 5.9 %collective-permute-start.19 = (bf16[80,128]{1,0:T(8,128)(2,1)S(1)}, bf16[80,128]{1,0:T(8,128)(2,1)S(1)}, u32[]{:S(2)}, u32[]{:S(2)}) collective-permute-start(bf16[80,128]{1,0:T(8,128)(2,1)S(1)} %collective-permute-done.18), channel_id=1, source_target_pairs={{0,1},{1,2},{2,3},{3,4},{4,5},{5,6},{6,7},{7,8},{8,9},{9,10},{10,1... | collective-permute-start | bytes 61448 | tf_op jit(solution)/shard_map/ppermute | solution.py:48
  145.1 5.9 %collective-permute-start.20 = (bf16[80,128]{1,0:T(8,128)(2,1)S(1)}, bf16[80,128]{1,0:T(8,128)(2,1)S(1)}, u32[]{:S(2)}, u32[]{:S(2)}) collective-permute-start(bf16[80,128]{1,0:T(8,128)(2,1)S(1)} %collective-permute-done.19), channel_id=1, source_target_pairs={{0,1},{1,2},{2,3},{3,4},{4,5},{5,6},{6,7},{7,8},{8,9},{9,10},{10,1... | collective-permute-start | bytes 61448 | tf_op jit(solution)/shard_map/ppermute | solution.py:48
  151.0 5.9 %collective-permute-start.21 = (bf16[80,128]{1,0:T(8,128)(2,1)S(1)}, bf16[80,128]{1,0:T(8,128)(2,1)S(1)}, u32[]{:S(2)}, u32[]{:S(2)}) collective-permute-start(bf16[80,128]{1,0:T(8,128)(2,1)S(1)} %collective-permute-done.20), channel_id=1, source_target_pairs={{0,1},{1,2},{2,3},{3,4},{4,5},{5,6},{6,7},{7,8},{8,9},{9,10},{10,1... | collective-permute-start | bytes 61448 | tf_op jit(solution)/shard_map/ppermute | solution.py:48
  156.9 5.9 %collective-permute-start.22 = (bf16[80,128]{1,0:T(8,128)(2,1)S(1)}, bf16[80,128]{1,0:T(8,128)(2,1)S(1)}, u32[]{:S(2)}, u32[]{:S(2)}) collective-permute-start(bf16[80,128]{1,0:T(8,128)(2,1)S(1)} %collective-permute-done.21), channel_id=1, source_target_pairs={{0,1},{1,2},{2,3},{3,4},{4,5},{5,6},{6,7},{7,8},{8,9},{9,10},{10,1... | collective-permute-start | bytes 61448 | tf_op jit(solution)/shard_map/ppermute | solution.py:48
  168.7 5.9 %collective-permute-start.24 = (bf16[80,128]{1,0:T(8,128)(2,1)S(1)}, bf16[80,128]{1,0:T(8,128)(2,1)S(1)}, u32[]{:S(2)}, u32[]{:S(2)}) collective-permute-start(bf16[80,128]{1,0:T(8,128)(2,1)S(1)} %collective-permute-done.23), channel_id=1, source_target_pairs={{0,1},{1,2},{2,3},{3,4},{4,5},{5,6},{6,7},{7,8},{8,9},{9,10},{10,1... | collective-permute-start | bytes 61448 | tf_op jit(solution)/shard_map/ppermute | solution.py:48
  174.6 5.9 %collective-permute-start.25 = (bf16[80,128]{1,0:T(8,128)(2,1)S(1)}, bf16[80,128]{1,0:T(8,128)(2,1)S(1)}, u32[]{:S(2)}, u32[]{:S(2)}) collective-permute-start(bf16[80,128]{1,0:T(8,128)(2,1)S(1)} %collective-permute-done.24), channel_id=1, source_target_pairs={{0,1},{1,2},{2,3},{3,4},{4,5},{5,6},{6,7},{7,8},{8,9},{9,10},{10,1... | collective-permute-start | bytes 61448 | tf_op jit(solution)/shard_map/ppermute | solution.py:48
  180.5 5.9 %collective-permute-start.26 = (bf16[80,128]{1,0:T(8,128)(2,1)S(1)}, bf16[80,128]{1,0:T(8,128)(2,1)S(1)}, u32[]{:S(2)}, u32[]{:S(2)}) collective-permute-start(bf16[80,128]{1,0:T(8,128)(2,1)S(1)} %collective-permute-done.25), channel_id=1, source_target_pairs={{0,1},{1,2},{2,3},{3,4},{4,5},{5,6},{6,7},{7,8},{8,9},{9,10},{10,1... | collective-permute-start | bytes 61448 | tf_op jit(solution)/shard_map/ppermute | solution.py:48
  186.4 5.9 %collective-permute-start.27 = (bf16[80,128]{1,0:T(8,128)(2,1)S(1)}, bf16[80,128]{1,0:T(8,128)(2,1)S(1)}, u32[]{:S(2)}, u32[]{:S(2)}) collective-permute-start(bf16[80,128]{1,0:T(8,128)(2,1)S(1)} %collective-permute-done.26), channel_id=1, source_target_pairs={{0,1},{1,2},{2,3},{3,4},{4,5},{5,6},{6,7},{7,8},{8,9},{9,10},{10,1... | collective-permute-start | bytes 61448 | tf_op jit(solution)/shard_map/ppermute | solution.py:48
  210.0 5.9 %collective-permute-start.31 = (bf16[80,128]{1,0:T(8,128)(2,1)S(1)}, bf16[80,128]{1,0:T(8,128)(2,1)S(1)}, u32[]{:S(2)}, u32[]{:S(2)}) collective-permute-start(bf16[80,128]{1,0:T(8,128)(2,1)S(1)} %collective-permute-done.30), channel_id=1, source_target_pairs={{0,1},{1,2},{2,3},{3,4},{4,5},{5,6},{6,7},{7,8},{8,9},{9,10},{10,1... | collective-permute-start | bytes 61448 | tf_op jit(solution)/shard_map/ppermute | solution.py:48
  (20 other events, 1257.3 us)
